TPU v7x, 512 devices: a whole 4x4x16 slice. The times are simulated.
512 devices in a mesh: sp: 64 (over z, y), dp: 8 (over x, core).
Axes of the slice: x: 4, y: 4, z: 16, core: 2. Of those that a mesh axis runs over, the one named last changes fastest.
Arguments:
- tokens: bfloat16 [8, 8192, 2048], P('dp', 'sp'), may hold values from -6 to 6
- w_value: bfloat16 [2048, 1024], P('dp', 'sp'), may hold values from -0.125 to 0.125
- w_gate: bfloat16 [2048, 1024], P('dp', 'sp'), may hold values from -0.125 to 0.125
- w_out: bfloat16 [1024, 2048], P('dp', 'sp'), may hold values from -0.1875 to 0.1875
- conv_taps: bfloat16 [1024, 31], replicated, may hold values from -1 to 1
- norm_gain: float32 [1024], replicated, may hold values from 0.1 to 1.9
- norm_bias: float32 [1024], replicated, may hold values from -3 to 3
Outputs:
- mixed: bfloat16 [8, 8192, 2048], P('dp', 'sp')
All inputs are finite; a program needn't handle non-finite values.
Results may differ from a plain program's by a relative error of at most 0.0064.
Values may be sent and summed in bfloat16 or wider, within the bound.
A program may use at most 64 MiB of HBM per device.

v0:
```python
import jax
import jax.numpy as jnp
from jax import lax
from jax.sharding import PartitionSpec as P


def in_order(pieces, dim):
    pieces = jnp.moveaxis(pieces, 0, dim)
    lengths = pieces.shape
    return pieces.reshape(*lengths[:dim], lengths[dim] * lengths[dim + 1], *lengths[dim + 2 :])


def one_gather(arrays, axis, dims):
    flat = jnp.concatenate([a.reshape(-1) for a in arrays])
    lines, at, finished = (lax.all_gather(flat, axis), 0, [])
    for a, dim in zip(arrays, dims):
        pieces = lines[:, at : at + a.size].reshape(-1, *a.shape)
        finished.append(in_order(pieces, dim))
        at += a.size
    return tuple(finished)


def in_one_piece(arrays, axis, dim, along):
    ends, at = ([], 0)
    for a in arrays[:-1]:
        at += a.shape[along]
        ends.append(at)
    both = jnp.concatenate(arrays, axis=along)
    return tuple(jnp.split(lax.all_gather(both, axis, axis=dim, tiled=True), ends, axis=along))


def padded_2(block, sides, width):
    for axis, dim in sides:
        count = lax.axis_size(axis)
        forward = [(i, i + 1) for i in range(count - 1)]
        backward = [(target, source) for source, target in forward]
        low = lax.ppermute(
            lax.slice_in_dim(block, block.shape[dim] - width, None, axis=dim), axis, forward
        )
        high = lax.ppermute(lax.slice_in_dim(block, 0, width, axis=dim), axis, backward)
        block = jnp.concatenate([low, block, high], axis=dim)
    return block


def depthwise(padded, taps, length):
    weights = taps.astype(jnp.float32)
    total = jnp.zeros((padded.shape[0], length), jnp.float32)
    for offset in range(taps.shape[1]):
        total = total + weights[:, offset : offset + 1] * padded[
            :, offset : offset + length
        ].astype(jnp.float32)
    return total.astype(jnp.bfloat16)


def normalize(conv_tok, norm_gain, norm_bias):
    values = lax.optimization_barrier(conv_tok).astype(jnp.float32)
    mean = jnp.mean(values, axis=0, keepdims=True)
    centred = values - mean
    variance = jnp.mean(centred * centred, axis=0, keepdims=True)
    normed = centred * lax.rsqrt(variance + 1e-05) * norm_gain[:, None] + norm_bias[:, None]
    return (normed * jax.nn.sigmoid(normed)).astype(jnp.bfloat16)


def on_device(tokens, w_value, w_gate, w_out, conv_taps, norm_gain, norm_bias):
    rows = tokens[0]
    contract_rows = (((0,), (1,)), ((), ()))
    contract_first = (((0,), (0,)), ((), ()))
    value_rows, gate_rows, out_rows = one_gather((w_value, w_gate, w_out), "sp", (1, 1, 1))
    pieces = in_one_piece((value_rows, gate_rows), "dp", 0, 1)
    part = rows
    value = lax.dot_general(pieces[0], part, contract_rows, preferred_element_type=jnp.float32)
    gate = lax.dot_general(pieces[1], part, contract_rows, preferred_element_type=jnp.float32)
    value, gate = (value, gate)
    gated_t = (value * jax.nn.sigmoid(gate)).astype(jnp.bfloat16)
    margin = conv_taps.shape[1] // 2
    padded = padded_2(gated_t, (("sp", 1),), margin)
    conv_tok = depthwise(padded, conv_taps, gated_t.shape[1])
    act_t = normalize(conv_tok, norm_gain, norm_bias)
    part = act_t
    mixed = lax.dot_general(
        part,
        lax.all_gather(out_rows, "dp", axis=0, tiled=True),
        contract_first,
        preferred_element_type=jnp.float32,
    )
    return mixed.astype(jnp.bfloat16)[None]


def solution(mesh):
    in_specs = (P("dp", "sp", None), P("dp", "sp"), P("dp", "sp"), P("dp", "sp"), P(), P(), P())
    out_specs = P("dp", "sp", None)
    return jax.shard_map(
        on_device, mesh=mesh, in_specs=in_specs, out_specs=out_specs, check_vma=False
    )
```

profile of v0, /device:TPU:1, one launch (start us, length us, event | category | flops | bytes accessed | tf_op | source)
XLA Modules:
  0.0 280.5 jit_solution(17725139445144940607)
XLA Ops:
  6.5 0.0 copy-start
  6.5 0.0 all-gather.9.cloned.1.call-start
  6.5 0.9 copy.23
  7.4 0.1 reshape.41
  7.5 0.8 copy.24
  8.3 0.1 reshape.42
  8.5 0.8 copy.25
  9.3 0.1 reshape.43
  9.4 0.6 pad_maximum_fusion.3
  10.0 0.0 all-gather.9.cloned.1.call-update
  10.0 0.0 all-gather.5.cloned.1.call-start
  10.1 136.0 %all-gather.9.cloned.1.call-done = bf16[786432]{0:T(1024)(128)(2,1)} async-done(((bf16[12288]{0:T(1024)(128)(2,1)}), bf16[786432]{0:T(1024)(128)(2,1)}) %all-gather.9.cloned.1.call-update) | async-done | bytes 1572880 | tf_op jit(solution)/shard_map/all_gather | solution.py:15
  146.1 2.5 reshape.50
  148.6 0.9 fusion.71
  149.5 1.5 copy.26
  151.1 1.3 copy.27
  152.4 0.5 copy.28
  152.9 0.0 copy-start.1
  152.9 1.3 copy.29
  154.2 1.1 pad_maximum_fusion
  155.4 0.0 all-gather.5.cloned.1.call-update
  155.4 0.0 all-gather.7.cloned.1.call-start
  155.4 0.5 copy.30
  155.9 2.3 copy.31
  158.2 0.0 all-gather.7.cloned.1.call-update
  158.3 0.0 copy-done.1
  158.3 0.1 fusion.73
  158.3 64.6 %all-gather.5.cloned.1.call-done = bf16[2048,2048]{0,1:T(8,128)(2,1)} async-done(((bf16[256,2048]{0,1:T(8,128)(2,1)}), bf16[2048,2048]{0,1:T(8,128)(2,1)}) %all-gather.5.cloned.1.call-update) | async-done | bytes 8388624 | tf_op jit(solution)/shard_map/all_gather | solution.py:29
  223.0 0.0 copy-done
  223.0 0.0 copy-start.2
  223.0 3.9 %fusion.20 = f32[1024,128]{0,1:T(8,128)S(1)} fusion(bf16[2048,2048]{0,1:T(8,128)(2,1)} %all-gather.5.cloned.1.call-done, bf16[1,128,2048]{2,1,0:T(8,128)(2,1)S(1)} %copy-done), kind=kOutput, calls=%fused_computation.39 | convolution fusion | flops 537264128 | bytes 5242880 | tf_op jit(solution)/shard_map/dot_general | solution.py:72
  226.9 0.7 copy-done.2
  227.6 0.0 copy-start.3
  227.6 0.0 copy-start.4
  227.6 1.5 fusion.17
  229.1 3.1 %collective-permute-start = (bf16[1024,15]{0,1:T(8,128)(2,1)S(1)}, bf16[1024,15]{0,1:T(8,128)(2,1)S(1)}, u32[]{:S(2)}, u32[]{:S(2)}) collective-permute-start(bf16[1024,15]{0,1:T(8,128)(2,1)S(1)} %get-tuple-element.8), channel_id=1, source_target_pairs={{0,8},{8,16},{16,24},{24,32},{32,40},{40,48},{48,56},{56,64},{64,7... | collective-permute-start | bytes 92168 | tf_op jit(solution)/shard_map/ppermute | solution.py:37
  232.3 1.3 collective-permute-start.1
  233.6 0.0 collective-permute-done
  233.7 3.3 %collective-permute-done.1 = bf16[1024,15]{0,1:T(8,128)(2,1)S(1)} collective-permute-done((bf16[1024,15]{0,1:T(8,128)(2,1)S(1)}, bf16[1024,15]{0,1:T(8,128)(2,1)S(1)}, u32[]{:S(2)}, u32[]{:S(2)}) %collective-permute-start.1) | collective-permute-done | bytes 30752 | tf_op jit(solution)/shard_map/ppermute | solution.py:40
  237.0 2.4 add_convert_fusion
  239.4 0.1 convert_reduce_fusion
  239.5 0.2 fusion.25
  239.7 29.6 %all-gather.7.cloned.1.call-done = bf16[1024,2048]{0,1:T(8,128)(2,1)} async-done(((bf16[128,2048]{0,1:T(8,128)(2,1)}), bf16[1024,2048]{0,1:T(8,128)(2,1)}) %all-gather.7.cloned.1.call-update) | async-done | bytes 4194320 | tf_op jit(solution)/shard_map/all_gather | solution.py:82
  269.4 0.0 copy-done.3
  269.4 0.0 copy-done.4
  269.4 4.6 %fusion.4 = bf16[1,128,2048]{2,1,0:T(8,128)(2,1)} fusion(bf16[1024,2048]{0,1:T(8,128)(2,1)} %all-gather.7.cloned.1.call-done, bf16[1024,128]{0,1:T(8,128)(2,1)S(1)} %add_convert_fusion, f32[1024]{0:T(1024)S(1)} %copy-done.3, f32[1024]{0:T(1024)S(1)} %copy-done.4, f32[128]{0:T(128)S(1)} %add_rsqrt_fusion, f32[128]{0:T(128)S(1)} %broadcast_multiply_fusion), kind=kOutput, calls=%fused_computation.5 | convolution fusion | flops 538443776 | bytes 4989952 | tf_op jit(solution)/shard_map/dot_general | solution.py:80
  (4 shorter events, 0.1 us)
Async XLA Ops:
  6.5 216.4 %copy-start = (bf16[1,128,2048]{2,1,0:T(8,128)(2,1)S(1)}, bf16[1,128,2048]{2,1,0:T(8,128)(2,1)}, u32[]{:S(2)}) copy-start(bf16[1,128,2048]{2,1,0:T(8,128)(2,1)} %param.7) | copy-start | bytes 1572868
  6.5 139.5 %all-gather.9.cloned.1.call-start = ((), (), s32[]{:S(2)}) async-start(), calls=%async_computation.2 | async-start | bytes 1597440 | tf_op jit(solution)/shard_map/all_gather | solution.py:15
  10.0 213.0 %all-gather.5.cloned.1.call-start = ((), (), s32[]{:S(2)}) async-start(), calls=%async_computation | async-start | bytes 9437184 | tf_op jit(solution)/shard_map/all_gather | solution.py:29
  152.9 5.4 %copy-start.1 = (bf16[1024,31]{0,1:T(8,128)(2,1)S(1)}, bf16[1024,31]{0,1:T(8,128)(2,1)}, u32[]{:S(2)}) copy-start(bf16[1024,31]{0,1:T(8,128)(2,1)} %param.11) | copy-start | bytes 190468
  155.4 114.0 %all-gather.7.cloned.1.call-start = ((), (), s32[]{:S(2)}) async-start(), calls=%async_computation.1 | async-start | bytes 4718592 | tf_op jit(solution)/shard_map/all_gather | solution.py:82
  223.0 4.6 %copy-start.2 = (bf16[2048,2048]{0,1:T(8,128)(2,1)S(1)}, bf16[2048,2048]{0,1:T(8,128)(2,1)}, u32[]{:S(2)}) copy-start(bf16[2048,2048]{0,1:T(8,128)(2,1)} %all-gather.5.cloned.1.call-done) | copy-start | bytes 25165828
  227.6 41.8 %copy-start.3 = (f32[1024]{0:T(1024)S(1)}, f32[1024]{0:T(1024)}, u32[]{:S(2)}) copy-start(f32[1024]{0:T(1024)} %param.13) | copy-start | bytes 12292
  227.6 41.8 %copy-start.4 = (f32[1024]{0:T(1024)S(1)}, f32[1024]{0:T(1024)}, u32[]{:S(2)}) copy-start(f32[1024]{0:T(1024)} %param.12) | copy-start | bytes 12292
  229.1 4.5 %collective-permute-start = (bf16[1024,15]{0,1:T(8,128)(2,1)S(1)}, bf16[1024,15]{0,1:T(8,128)(2,1)S(1)}, u32[]{:S(2)}, u32[]{:S(2)}) collective-permute-start(bf16[1024,15]{0,1:T(8,128)(2,1)S(1)} %get-tuple-element.8), channel_id=1, source_target_pairs={{0,8},{8,16},{16,24},{24,32},{32,40},{40,48},{48,56},{56,64},{64,7... | collective-permute-start | bytes 92168 | tf_op jit(solution)/shard_map/ppermute | solution.py:37
  232.3 4.7 %collective-permute-start.1 = (bf16[1024,15]{0,1:T(8,128)(2,1)S(1)}, bf16[1024,15]{0,1:T(8,128)(2,1)S(1)}, u32[]{:S(2)}, u32[]{:S(2)}) collective-permute-start(bf16[1024,15]{0,1:T(8,128)(2,1)S(1)} %get-tuple-element.9), channel_id=1, source_target_pairs={{8,0},{16,8},{24,16},{32,24},{40,32},{48,40},{56,48},{64,56},{72,6... | collective-permute-start | bytes 92168 | tf_op jit(solution)/shard_map/ppermute | solution.py:40
Sparse Core Ops, SparseCore 0:
  10.3 135.7 all-gather.8
  155.5 67.4 all-gather.4
  225.1 44.2 all-gather.6
where the time goes:
time: 281 us
  waiting for transfers between devices  234 us (83%)
  local copies, waits for them, and re-layouts  14.6 us (5%)
  between operations  13.2 us (5%)
  matrix products  10 us (4%)
  starting transfers between devices  4.52 us (2%)
  other arithmetic  4.51 us (2%)
    all_gather x1, waiting for transfers between devices, one_gather(): lines, at, finished = (lax.all_gather(flat, axis), 0, [])  136 us
    all_gather x1, waiting for transfers between devices, in_one_piece(): lax.all_gather(both, axis, axis=dim, tiled=True)  64.6 us
    all_gather x1, waiting for transfers between devices, on_device(): lax.all_gather(out_rows, 'dp', axis=0, tiled=True)  29.6 us
  transfers between devices with their start and end apart: 5, of which 4 were waited for; matrix products, arithmetic and copies ran while one was open for 4% of the time, Pallas kernels for 0%

commit v1 on v0

v1 whole, which is shorter than its diff:
```python
import jax
import jax.numpy as jnp
from jax import lax
from jax.experimental import pallas as pl
from jax.experimental.pallas import tpu as pltpu
from jax.sharding import PartitionSpec as P

MESH = pl.DeviceIdType.MESH
NSEM = 240
NT = (((1,), (1,)), ((), ()))


def kernel(tok, wv, wg, wo, taps, gain, bias, out, W, O, X, T, CV, ACT, ssem, rsem, lsem):
    sp = lax.axis_index("sp")
    dp = lax.axis_index("dp")
    z, y = sp // 4, lax.rem(sp, 4)
    x, c = dp // 2, lax.rem(dp, 2)
    q, r = z // 4, lax.rem(z, 4)

    def dev(x=x, y=y, z=z, c=c):
        return {"sp": z * 4 + y, "dp": x * 2 + c}

    def mod(v, n):
        return lax.rem(v + n, n)

    xl, xr = mod(x - 1, 4), mod(x + 1, 4)
    yl, yr = mod(y - 1, 4), mod(y + 1, 4)
    zl, zr = mod(z - 1, 16), mod(z + 1, 16)
    z4l, z4r = mod(z - 4, 16), mod(z + 4, 16)
    peers = [q * 4 + mod(r + d, 4) for d in (1, 2, 3)]
    qs = [q, mod(q - 1, 4), mod(q + 1, 4), mod(q + 2, 4)]
    prev, nxt = mod(sp - 1, 64), mod(sp + 1, 64)

    local = [
        pltpu.make_async_copy(wv, W.at[x, c, q, r, y, 0], lsem.at[0]),
        pltpu.make_async_copy(wg, W.at[x, c, q, r, y, 1], lsem.at[1]),
        pltpu.make_async_copy(wo, O.at[x, c, z, y], lsem.at[2]),
        pltpu.make_async_copy(tok, X.at[pl.ds(16, 128)], lsem.at[3]),
    ]
    for d in local:
        d.start()

    barrier = pltpu.get_barrier_semaphore()
    partners = [dev(x=xl), dev(x=xr), dev(y=yl), dev(y=yr), dev(z=zl), dev(z=zr), dev(z=z4l), dev(z=z4r)]
    partners += [dev(z=p) for p in peers]
    partners += [dev(c=1 - c), {"sp": prev, "dp": dp}, {"sp": nxt, "dp": dp}]
    for p in partners:
        pl.semaphore_signal(barrier, inc=1, device_id=p, device_id_type=MESH)

    T[...] = taps[...].astype(jnp.float32)

    @pl.when(sp == 0)
    def _():
        X[pl.ds(0, 16), :] = jnp.zeros((16, 2048), jnp.bfloat16)

    @pl.when(sp == 63)
    def _():
        X[pl.ds(144, 16), :] = jnp.zeros((16, 2048), jnp.bfloat16)

    pl.semaphore_wait(barrier, len(partners))
    for d in local:
        d.wait()

    sends = []
    count = [0]

    def describe(src, dst, to):
        i = count[0]
        count[0] += 1
        return pltpu.make_async_remote_copy(
            src_ref=src, dst_ref=dst, send_sem=ssem.at[i], recv_sem=rsem.at[i],
            device_id=to, device_id_type=MESH,
        )

    def send(ref, to):
        d = describe(ref, ref, to)
        d.start()
        sends.append(d)
        return d

    events = []
    st = {}

    def at(t):
        def add(f):
            events.append((t, len(events), f))
        return add

    halo_r = describe(X.at[pl.ds(128, 16)], X.at[pl.ds(0, 16)], {"sp": nxt, "dp": dp})
    halo_l = describe(X.at[pl.ds(16, 16)], X.at[pl.ds(144, 16)], {"sp": prev, "dp": dp})

    @at(0.9)
    def _():
        @pl.when(sp < 63)
        def _():
            halo_r.start()

        @pl.when(sp > 0)
        def _():
            halo_l.start()

    @at(0.1)
    def _():
        b = O.at[x, c, z, y]
        st["ox"] = (send(b, dev(x=xr)), send(b, dev(x=xl)))

    @at(2.4)
    def _():
        a, b = st["ox"]
        a.wait_recv()
        e = send(O.at[xl, c, z, y, pl.ds(0, 16)], dev(x=xr))
        b.wait_recv()
        st["ox2"] = (e, send(O.at[xr, c, z, y, pl.ds(16, 16)], dev(x=xl)))

    @at(4.7)
    def _():
        for d in st["ox2"]:
            d.wait_recv()
        b = O.at[:, c, z, y]
        st["oy"] = (send(b, dev(y=yr)), send(b, dev(y=yl)))

    @at(7.2)
    def _():
        a, b = st["oy"]
        a.wait_recv()
        e = send(O.at[pl.ds(0, 2), c, z, yl], dev(y=yr))
        b.wait_recv()
        st["oy2"] = (e, send(O.at[pl.ds(2, 2), c, z, yr], dev(y=yl)))

    def ring_sends(s):
        zo, zp = mod(z - s, 16), mod(z + s, 16)
        for h in (0, 1):
            if s < 8:
                st["r", s, h] = send(O.at[:, c, zo, pl.ds(2 * h, 2)], dev(z=zr))
            if s < 7:
                st["l", s, h] = send(O.at[:, c, zp, pl.ds(2 * h, 2)], dev(z=zl))

    @at(9.6)
    def _():
        for d in st["oy2"]:
            d.wait_recv()
        ring_sends(0)
        st["od", 0] = [send(O.at[:, c, z], dev(c=1 - c))]

    def ring(s):
        zo, zp = mod(z - s, 16), mod(z + s, 16)
        for h in (0, 1):
            st["r", s - 1, h].wait_recv()
            if s < 8:
                st["r", s, h] = send(O.at[:, c, zo, pl.ds(2 * h, 2)], dev(z=zr))
            if s < 8:
                st["l", s - 1, h].wait_recv()
            if s < 7:
                st["l", s, h] = send(O.at[:, c, zp, pl.ds(2 * h, 2)], dev(z=zl))
        st["od", s] = [send(O.at[:, c, zo], dev(c=1 - c))]
        if s < 8:
            st["od", s].append(send(O.at[:, c, zp], dev(c=1 - c)))

    for s in range(1, 9):
        at(10 + 3.3 * s)(lambda s=s: ring(s))

    @at(0.0)
    def _():
        b = W.at[x, c, q, r, y]
        st["s2", 0] = [send(b, dev(z=p)) for p in peers]
        st["s1"] = (send(b, dev(z=z4r)), send(b, dev(z=z4l)))

    @at(4.2)
    def _():
        a, b = st["s1"]
        a.wait_recv()
        e = send(W.at[x, c, qs[1], r, y, 0], dev(z=z4r))
        b.wait_recv()
        st["s1b"] = (e, send(W.at[x, c, qs[2], r, y, 1], dev(z=z4l)))
        for m in (1, 2):
            st["s2", m] = [send(W.at[x, c, qs[m], r, y], dev(z=p)) for p in peers]

    @at(8.2)
    def _():
        for d in st["s1b"]:
            d.wait_recv()
        st["s2", 3] = [send(W.at[x, c, qs[3], r, y], dev(z=p)) for p in peers]

    def p1(m):
        for d in st["s2", m]:
            d.wait_recv()
        A, B = W.at[x, c, qs[m], :, y, 0], W.at[x, c, qs[m], :, y, 1]
        st["p1", m] = (send(A, dev(y=yr)), send(A, dev(y=yl)), send(B, dev(x=xr)), send(B, dev(x=xl)))

    def p1r(m):
        a, b, e, f = st["p1", m]
        lo, hi = pl.ds(0, 2), pl.ds(2, 2)
        a.wait_recv()
        g = [send(W.at[x, c, qs[m], lo, yl, 0], dev(y=yr))]
        b.wait_recv()
        g.append(send(W.at[x, c, qs[m], hi, yr, 0], dev(y=yl)))
        e.wait_recv()
        g.append(send(W.at[xl, c, qs[m], lo, y, 1], dev(x=xr)))
        f.wait_recv()
        g.append(send(W.at[xr, c, qs[m], hi, y, 1], dev(x=xl)))
        st["p1r", m] = g

    def p2(m):
        for d in st["p1r", m]:
            d.wait_recv()
        A, B = W.at[x, c, qs[m], :, :, 0], W.at[:, c, qs[m], :, y, 1]
        st["p2", m] = (send(A, dev(x=xr)), send(A, dev(x=xl)), send(B, dev(y=yr)), send(B, dev(y=yl)))

    def p2r(m):
        a, b, e, f = st["p2", m]
        lo, hi = pl.ds(0, 2), pl.ds(2, 2)
        a.wait_recv()
        g = [send(W.at[xl, c, qs[m], lo, :, 0], dev(x=xr))]
        b.wait_recv()
        g.append(send(W.at[xr, c, qs[m], hi, :, 0], dev(x=xl)))
        e.wait_recv()
        g.append(send(W.at[:, c, qs[m], lo, yl, 1], dev(y=yr)))
        f.wait_recv()
        g.append(send(W.at[:, c, qs[m], hi, yr, 1], dev(y=yl)))
        st["p2r", m] = g

    def d2d(m):
        for d in st["p2r", m]:
            d.wait_recv()
        st["d2d", m] = [send(W.at[:, c, qs[m], :, :, k], dev(c=1 - c)) for k in (0, 1)]

    def compute(m):
        for d in st["d2d", m]:
            d.wait_recv()
        if m == 0:
            @pl.when(sp > 0)
            def _():
                halo_r.wait_recv()

            @pl.when(sp < 63)
            def _():
                halo_l.wait_recv()

        qm = qs[m]
        acc = [None, None]
        for i in range(8):
            xs = X[:, 256 * i : 256 * i + 256]
            for k in (0, 1):
                w = W[i // 2, i % 2, qm, :, :, k].reshape(256, 256)
                part = lax.dot_general(xs, w, NT, preferred_element_type=jnp.float32)
                acc[k] = part if acc[k] is None else acc[k] + part
        gated = (acc[0] * jax.nn.sigmoid(acc[1])).astype(jnp.bfloat16).astype(jnp.float32)
        for h in (0, 1):
            strip = gated[:, 128 * h : 128 * h + 128]
            lanes = pl.ds(pl.multiple_of(qm * 256 + 128 * h, 128), 128)
            total = jnp.zeros((128, 128), jnp.float32)
            for shift in range(8):
                rolled = strip if shift == 0 else pltpu.roll(strip, 160 - shift, 0)
                for k in range(31):
                    if (k + 1) % 8 == shift:
                        first = (k + 1) // 8 * 8
                        total = total + T[pl.ds(k, 1), lanes] * rolled[first : first + 128]
            CV[:, lanes] = total.astype(jnp.bfloat16).astype(jnp.float32)

    t1 = [3.4, 7.6, 7.7, 11.4]
    t2 = [8.1, 12.6, 13.2, 16.4]
    t3 = [13.5, 17.8, 22.0, 26.2]
    for m in range(4):
        at(t1[m])(lambda m=m: p1(m))
        at(t1[m] + 2.3)(lambda m=m: p1r(m))
        at(t2[m])(lambda m=m: p2(m))
        at(t3[m])(lambda m=m: p2r(m))
        at(t3[m] + 3.9)(lambda m=m: d2d(m))
        at(t3[m] + 5.6)(lambda m=m: compute(m))

    for _, _, f in sorted(events, key=lambda e: e[:2]):
        f()

    def norm(i, carry):
        rows = pl.ds(pl.multiple_of(i * 16, 16), 16)
        v = CV[rows, :]
        mean = jnp.mean(v, axis=-1, keepdims=True)
        cen = v - mean
        var = jnp.mean(cen * cen, axis=-1, keepdims=True)
        n = cen * lax.rsqrt(var + 1e-05) * gain[...] + bias[...]
        ACT[rows, :] = (n * jax.nn.sigmoid(n)).astype(jnp.bfloat16)
        return carry

    lax.fori_loop(0, 8, norm, 0)

    for s in range(9):
        for d in st["od", s]:
            d.wait_recv()

    def project(j, carry):
        acc = None
        zs = pl.ds(j * 4, 4)
        for i in range(4):
            w = jnp.concatenate([O[i, 0, zs].reshape(512, 128), O[i, 1, zs].reshape(512, 128)], axis=1)
            part = lax.dot_general(
                ACT[:, 256 * i : 256 * i + 256], w, NT, preferred_element_type=jnp.float32
            )
            acc = part if acc is None else acc + part
        out[:, pl.ds(pl.multiple_of(j * 512, 512), 512)] = acc.astype(jnp.bfloat16)
        return carry

    lax.fori_loop(0, 4, project, 0)

    for d in sends:
        d.wait_send()

    @pl.when(sp < 63)
    def _():
        halo_r.wait_send()

    @pl.when(sp > 0)
    def _():
        halo_l.wait_send()


def on_device(tokens, w_value, w_gate, w_out, conv_taps, norm_gain, norm_bias):
    hbm = pl.BlockSpec(memory_space=pl.ANY)
    vmem = pl.BlockSpec(memory_space=pltpu.VMEM)
    mixed = pl.pallas_call(
        kernel,
        out_shape=jax.ShapeDtypeStruct((128, 2048), jnp.bfloat16),
        in_specs=[hbm] * 4 + [vmem] * 3,
        out_specs=vmem,
        scratch_shapes=[
            pltpu.VMEM((4, 2, 4, 4, 4, 2, 16, 256), jnp.bfloat16),
            pltpu.VMEM((4, 2, 16, 4, 32, 128), jnp.bfloat16),
            pltpu.VMEM((160, 2048), jnp.bfloat16),
            pltpu.VMEM((31, 1024), jnp.float32),
            pltpu.VMEM((128, 1024), jnp.float32),
            pltpu.VMEM((128, 1024), jnp.bfloat16),
            pltpu.SemaphoreType.DMA((NSEM,)),
            pltpu.SemaphoreType.DMA((NSEM,)),
            pltpu.SemaphoreType.DMA((4,)),
        ],
        compiler_params=pltpu.CompilerParams(
            collective_id=0, has_side_effects=True, vmem_limit_bytes=48 * 1024 * 1024
        ),
    )(
        tokens[0],
        w_value.T,
        w_gate.T,
        w_out.T,
        conv_taps.T,
        norm_gain[None, :],
        norm_bias[None, :],
    )
    return mixed[None]


def solution(mesh):
    in_specs = (P("dp", "sp", None), P("dp", "sp"), P("dp", "sp"), P("dp", "sp"), P(), P(), P())
    out_specs = P("dp", "sp", None)
    return jax.shard_map(
        on_device, mesh=mesh, in_specs=in_specs, out_specs=out_specs, check_vma=False
    )
```

time: 281 us -> 81.5 us (0.29)
  waiting for transfers between devices: 234 us -> 0 us
  Pallas kernels: 0 us -> 75.7 us
  between operations: 13.2 us -> 0.02 us
  matrix products: 10 us -> 0 us
  local copies, waits for them, and re-layouts: 14.6 us -> 5.46 us
  starting transfers between devices: 4.52 us -> 0 us
  other arithmetic: 4.51 us -> 0 us
    all_gather x3 -> x0, waiting for transfers between devices: 230 us -> none  [the longest x1 136 us: one_gather(): lines, at, finished = (lax.all_gather(flat, axis), 0, [])]
    pallas_call x0 -> x1, Pallas kernels: none -> 75.7 us  [on_device(): pl.pallas_call(kernel, out_shape=jax.ShapeDtypeStruct((128, 2048), jnp.bf...]
    dot_general x3 -> x0, matrix products: 10 us -> none  [the longest x1 4.62 us: on_device(): lax.dot_general(part, lax.all_gather(out_rows, 'dp', axis=0, tiled=True),...]
    transpose x3 -> x0, local copies, waits for them, and re-layouts: 5 us -> none  [in_order(): pieces = jnp.moveaxis(pieces, 0, dim)]
    ppermute x2 -> x0, starting transfers between devices: 4.44 us -> none  [the longest x1 3.14 us: padded_2(): lax.ppermute(lax.slice_in_dim(block, block.shape[dim] - width, None, axis...]
    slice x7 -> x0, local copies, waits for them, and re-layouts: 3.51 us -> none  [the longest x4 3.4 us: one_gather(): pieces = lines[:, at:at + a.size].reshape(-1, *a.shape)]
    ppermute x2 -> x0, waiting for transfers between devices: 3.3 us -> none  [the longest x1 3.3 us: padded_2(): lax.ppermute(lax.slice_in_dim(block, 0, width, axis=dim), axis, backward)]
  transfers between devices with their start and end apart: 5 -> 0, of which waited for: 4 -> 0; matrix products, arithmetic and copies ran while one was open for 4% -> 0% of each run, Pallas kernels for 0% -> 0%
where the time goes in v1:
time: 81.5 us; the launch traced here: 81.2 us
  Pallas kernels  75.7 us (93%)
  local copies, waits for them, and re-layouts  5.46 us (7%)
    pallas_call x1, Pallas kernels, on_device(): pl.pallas_call(kernel, out_shape=jax.ShapeDtypeStruct((128, 2048), jnp.bf...  75.7 us
    unnamed x15, local copies, waits for them, and re-layouts  5.46 us

profile of v1, /device:TPU:1, one launch (start us, length us, event | category | flops | bytes accessed | tf_op | source)
XLA Modules:
  0.0 81.2 jit_solution(3930635815204108158)
XLA Ops:
  0.0 0.0 copy-start.2
  0.0 0.0 copy-start.5
  0.0 0.7 copy-done.2
  0.7 0.0 copy-done.5
  0.7 0.0 copy-start
  0.7 1.0 %copy-done = bf16[1,128,2048]{2,1,0:T(8,128)(2,1)S(1)} copy-done((bf16[1,128,2048]{2,1,0:T(8,128)(2,1)S(1)}, bf16[1,128,2048]{2,1,0:T(8,128)(2,1)}, u32[]{:S(2)}) %copy-start) | copy-done | bytes 524312
  1.7 0.0 copy-start.1
  1.7 0.8 %copy-done.1 = bf16[1024,31]{0,1:T(8,128)(2,1)S(1)} copy-done((bf16[1024,31]{0,1:T(8,128)(2,1)S(1)}, bf16[1024,31]{0,1:T(8,128)(2,1)}, u32[]{:S(2)}) %copy-start.1) | copy-done | bytes 63512
  2.6 0.0 copy-start.3
  2.6 0.7 copy-done.3
  3.3 0.0 copy-start.4
  3.3 0.7 copy-done.4
  4.0 0.0 copy-start.6
  4.0 0.7 copy-done.6
  4.7 75.7 %shard_map.73 = bf16[128,2048]{1,0:T(8,128)(2,1)S(1)} custom-call(bf16[128,2048]{1,0:T(8,128)(2,1)S(1)} %bitcast.9, bf16[16,256]{1,0:T(8,128)(2,1)S(1)} %bitcast.11, bf16[16,256]{1,0:T(8,128)(2,1)S(1)} %bitcast.12, bf16[32,128]{1,0:T(8,128)(2,1)S(1)} %bitcast.13, bf16[31,1024]{1,0:T(8,128)(2,1)S(1)} %bitcast.10, f32[1,1024]{1,0:T(1,128)S(1)} %bitcast.14, ...), custom_call_target="tpu_custom_call" | custom-call | tf_op jit(solution)/shard_map/pallas_call | solution.py:319
  80.4 0.8 copy.9
Async XLA Ops:
  0.0 0.7 copy-start.2
  0.0 0.7 copy-start.5
  0.7 1.0 %copy-start = (bf16[1,128,2048]{2,1,0:T(8,128)(2,1)S(1)}, bf16[1,128,2048]{2,1,0:T(8,128)(2,1)}, u32[]{:S(2)}) copy-start(bf16[1,128,2048]{2,1,0:T(8,128)(2,1)} %param.7) | copy-start | bytes 1572868
  1.7 0.8 %copy-start.1 = (bf16[1024,31]{0,1:T(8,128)(2,1)S(1)}, bf16[1024,31]{0,1:T(8,128)(2,1)}, u32[]{:S(2)}) copy-start(bf16[1024,31]{0,1:T(8,128)(2,1)} %param.11) | copy-start | bytes 190468
  2.6 0.7 copy-start.3
  3.3 0.7 copy-start.4
  4.0 0.7 copy-start.6

commit v2 on v1

v2 whole, which is shorter than its diff:
```python
import jax
import jax.numpy as jnp
from jax import lax
from jax.experimental import pallas as pl
from jax.experimental.pallas import tpu as pltpu
from jax.sharding import PartitionSpec as P

MESH = pl.DeviceIdType.MESH
NSEM = 100
ORDER = [
    "ox", "s1", "halo", "oxr+", "oxr-", "oy", "p1_0", "s1l", "s1r", "oyr+", "oyr-", "p1rA0+", "p1rA0-",
    "p1rB0+", "p1rB0-", "g0", "p2A_0", "p1_1", "s1rr", "p2B_0", "p1_2", "p1rA1+", "g1_0", "p2rA0+", "g1_1",
    "p1rB1+", "p1rB1-", "g1_3", "p2rA0-", "p2rB0+", "p1rA2-", "p1rA2+", "p1rB2+", "g1_2", "g2_0", "p1rA1-",
    "p1rB2-", "p1_3", "g2_3", "p2B_1", "g2_1", "dA_0", "g2_2", "p2A_2", "g3_0", "p2rB0-", "g3_3", "p1rA3-",
    "p2B_2", "p2A_1", "g3_1", "p1rA3+", "p2rB1-", "g3_2", "p1rB3+", "p1rB3-", "g4_0", "dB_0", "g4_3",
    "p2rA2+", "p2rB1+", "p2A_3", "g4_1", "p2rA1+", "p2rA1-", "g4_2", "p2B_3", "p2rB2-", "g5_3", "g5_0",
    "p2rA2-", "g5_1", "p2rB2+", "p2rA3-", "p2rA3+", "g5_2", "p2rB3+", "p2rB3-", "c_0", "dB_1", "dA_1", "g6_3",
    "g6_0", "dA_2", "g6_1", "dB_2", "g6_2", "dA_3", "dB_3", "g7_3", "c_1", "g7_0", "g7_1", "c_2", "g7_2",
    "g8_3", "c_3", "g8_1", "g8_0", "g8_2",
]
SENDS = {"ox+": "ox", "ox-": "ox", "oxr": "ox", "oy+": "oy", "oy-": "oy", "oyr": "oy",
         "s1+": "s1", "s1-": "s1", "s1r": "s1", "od": "od"}
FIRST = 0
NT = (((1,), (1,)), ((), ()))


def kernel(
    tok, wv, wg, wo, taps_in, gain_in, bias_in, result,
    out, W, O, X, TB, T, gain, bias, CV, ACT, ssem, rsem, lsem,
):
    sp = lax.axis_index("sp")
    dp = lax.axis_index("dp")
    z, y = sp // 4, lax.rem(sp, 4)
    x, c = dp // 2, lax.rem(dp, 2)
    q, r = z // 4, lax.rem(z, 4)

    def dev(x=x, y=y, z=z, c=c):
        return {"sp": z * 4 + y, "dp": x * 2 + c}

    def mod(v, n):
        return lax.rem(v + n, n)

    xl, xr = mod(x - 1, 4), mod(x + 1, 4)
    yl, yr = mod(y - 1, 4), mod(y + 1, 4)
    zl, zr = mod(z - 1, 16), mod(z + 1, 16)
    z4l, z4r = mod(z - 4, 16), mod(z + 4, 16)
    peers = [q * 4 + mod(r + d, 4) for d in (1, 2, 3)]
    qs = [q, mod(q - 1, 4), mod(q + 1, 4), mod(q + 2, 4)]
    prev, nxt = mod(sp - 1, 64), mod(sp + 1, 64)

    local = [
        pltpu.make_async_copy(wv, W.at[x, c, q, r, y, 0], lsem.at[0]),
        pltpu.make_async_copy(wg, W.at[x, c, q, r, y, 1], lsem.at[1]),
        pltpu.make_async_copy(wo, O.at[x, c, z, y], lsem.at[2]),
        pltpu.make_async_copy(tok, X.at[pl.ds(16, 128)], lsem.at[3]),
        pltpu.make_async_copy(taps_in, TB, lsem.at[4]),
        pltpu.make_async_copy(gain_in, gain, lsem.at[5]),
        pltpu.make_async_copy(bias_in, bias, lsem.at[6]),
    ]
    for d in local:
        d.start()

    barrier = pltpu.get_barrier_semaphore()
    partners = [dev(x=xl), dev(x=xr), dev(y=yl), dev(y=yr), dev(z=zl), dev(z=zr), dev(z=z4l), dev(z=z4r)]
    partners += [dev(z=p) for p in peers]
    partners += [dev(c=1 - c), {"sp": prev, "dp": dp}, {"sp": nxt, "dp": dp}]
    for p in partners:
        pl.semaphore_signal(barrier, inc=1, device_id=p, device_id_type=MESH)

    @pl.when(sp == 0)
    def _():
        X[pl.ds(0, 16), :] = jnp.zeros((16, 2048), jnp.bfloat16)

    @pl.when(sp == 63)
    def _():
        X[pl.ds(144, 16), :] = jnp.zeros((16, 2048), jnp.bfloat16)

    with jax.named_scope("barrier"):
        for d in local:
            d.wait()
        pl.semaphore_wait(barrier, len(partners))

    groups = {}

    kinds = {}

    def describe(src, dst, to, key, kind):
        i = groups.setdefault(key, len(groups))
        j = kinds.setdefault(kind, len(kinds))
        return pltpu.make_async_remote_copy(
            src_ref=src, dst_ref=dst, send_sem=ssem.at[j], recv_sem=rsem.at[i],
            device_id=to, device_id_type=MESH,
        )

    def send(key, ref, to):
        kind = key[0] if isinstance(key, tuple) else SENDS[key]
        describe(ref, ref, to, key, kind).start()

    def arrived(key, ref):
        describe(ref, ref, dev(c=1 - c), key, "d2d").wait_recv()

    def sent(kind, ref):
        describe(ref, ref, dev(c=1 - c), "od", kind).wait_send()

    events = {}

    def event(name):
        def add(f):
            events[name] = f
        return add

    halo_r = describe(X.at[pl.ds(128, 16)], X.at[pl.ds(0, 16)], {"sp": nxt, "dp": dp}, "hr", "hr")
    halo_l = describe(X.at[pl.ds(16, 16)], X.at[pl.ds(144, 16)], {"sp": prev, "dp": dp}, "hl", "hl")
    lo, hi = pl.ds(0, 2), pl.ds(2, 2)

    @event("halo")
    def _():
        @pl.when(sp < 63)
        def _():
            halo_r.start()

        @pl.when(sp > 0)
        def _():
            halo_l.start()

        T[...] = TB[...].astype(jnp.float32)

    @event("ox")
    def _():
        send("ox+", O.at[x, c, z, y], dev(x=xr))
        send("ox-", O.at[x, c, z, y], dev(x=xl))

    @event("oxr+")
    def _():
        arrived("ox+", O.at[x, c, z, y])
        send("oxr", O.at[xl, c, z, y, pl.ds(0, 16)], dev(x=xr))

    @event("oxr-")
    def _():
        arrived("ox-", O.at[x, c, z, y])
        send("oxr", O.at[xr, c, z, y, pl.ds(16, 16)], dev(x=xl))

    @event("oy")
    def _():
        arrived("oxr", O.at[x, c, z, y])
        send("oy+", O.at[:, c, z, y], dev(y=yr))
        send("oy-", O.at[:, c, z, y], dev(y=yl))

    @event("oyr+")
    def _():
        arrived("oy+", O.at[:, c, z, y])
        send("oyr", O.at[lo, c, z, yl], dev(y=yr))

    @event("oyr-")
    def _():
        arrived("oy-", O.at[:, c, z, y])
        send("oyr", O.at[hi, c, z, yr], dev(y=yl))

    stepped = [0] * 9

    def ring(s, h):
        zo, zp = mod(z - s, 16), mod(z + s, 16)
        if s > 0:
            arrived(("ring", s - 1, h), O.at[:, c, z, pl.ds(0, 2 if s < 8 else 1)])
        if s < 8:
            send(("ring", s, h), O.at[:, c, zo, h], dev(z=zr))
        if s < 7:
            send(("ring", s, h), O.at[:, c, zp, h], dev(z=zl))
        stepped[s] += 1
        if stepped[s] == 4:
            send("od", O.at[:, c, zo], dev(c=1 - c))
            if 0 < s < 8:
                send("od", O.at[:, c, zp], dev(c=1 - c))

    @event("g0")
    def _():
        arrived("oyr", O.at[:, c, z, y])
        for h in range(4):
            ring(0, h)

    for s in range(1, 9):
        for h in range(4):
            event(f"g{s}_{h}")(lambda s=s, h=h: ring(s, h))

    def s2(m):
        for p in peers:
            send(("s2", m), W.at[x, c, qs[m], r, y], dev(z=p))

    @event("s1")
    def _():
        s2(0)
        send("s1+", W.at[x, c, q, r, y], dev(z=z4r))
        send("s1-", W.at[x, c, q, r, y], dev(z=z4l))

    @event("s1l")
    def _():
        arrived("s1+", W.at[x, c, q, r, y])
        send("s1r", W.at[x, c, qs[1], r, y, 0], dev(z=z4r))
        s2(1)

    @event("s1r")
    def _():
        arrived("s1-", W.at[x, c, q, r, y])
        send("s1r", W.at[x, c, qs[2], r, y, 1], dev(z=z4l))
        s2(2)

    @event("s1rr")
    def _():
        arrived("s1r", W.at[x, c, q, r, y])
        s2(3)

    yn, xn = {"+": dev(y=yr), "-": dev(y=yl)}, {"+": dev(x=xr), "-": dev(x=xl)}
    at = {"o": 0, "+": -1, "-": 1, "x": 2}

    def part(T, m, p, rows=slice(None)):
        if T == "A":
            return W.at[x, c, qs[m], rows, mod(y + at[p], 4), 0]
        return W.at[mod(x + at[p], 4), c, qs[m], rows, y, 1]

    def slab(T, m, d, rows=slice(None)):
        if T == "A":
            return W.at[mod(x + at[d], 4), c, qs[m], rows, :, 0]
        return W.at[:, c, qs[m], rows, mod(y + at[d], 4), 1]

    ring1, ring2 = {"A": yn, "B": xn}, {"A": xn, "B": yn}
    half = {"+": lo, "-": hi}

    def p1(m):
        arrived(("s2", m), W.at[x, c, qs[m], pl.ds(0, 3), y])
        for T in "AB":
            for d in "+-":
                send(("p1", T, m, d), part(T, m, "o"), ring1[T][d])
            for d in "+-":
                send(("p2", T, m, d), part(T, m, "o"), ring2[T][d])

    def p1r(T, m, d):
        arrived(("p1", T, m, d), part(T, m, "o"))
        send(("p1r", T, m), part(T, m, d, half[d]), ring1[T][d])
        for e in "+-":
            send(("p2", T, m, e), part(T, m, d), ring2[T][e])

    def p2(T, m):
        arrived(("p1r", T, m), part(T, m, "o"))
        for e in "+-":
            send(("p2", T, m, e), part(T, m, "x"), ring2[T][e])
        send(("d2d", m), slab(T, m, "o"), dev(c=1 - c))

    def p2r(T, m, d):
        arrived(("p2", T, m, d), slab(T, m, d))
        send(("p2r", T, m), slab(T, m, d, half[d]), ring2[T][d])
        send(("d2d", m), slab(T, m, d), dev(c=1 - c))

    def d2d(T, m):
        arrived(("p2r", T, m), slab(T, m, "+"))
        send(("d2d", m), slab(T, m, "x"), dev(c=1 - c))

    def compute(m):
        arrived(("d2d", m), W.at[:, 1 - c, qs[m]])
        if m == FIRST:
            @pl.when(sp > 0)
            def _():
                halo_r.wait_recv()

            @pl.when(sp < 63)
            def _():
                halo_l.wait_recv()

        qm = qs[m]
        acc = [None, None]
        for i in range(8):
            xs = X[:, 256 * i : 256 * i + 256]
            for k in (0, 1):
                w = W[i // 2, i % 2, qm, :, :, k].reshape(256, 256)
                part = lax.dot_general(xs, w, NT, preferred_element_type=jnp.float32)
                acc[k] = part if acc[k] is None else acc[k] + part
        gated = (acc[0] * jax.nn.sigmoid(acc[1])).astype(jnp.bfloat16).astype(jnp.float32)
        for h in (0, 1):
            strip = gated[:, 128 * h : 128 * h + 128]
            lanes = pl.ds(pl.multiple_of(qm * 256 + 128 * h, 128), 128)
            total = jnp.zeros((128, 128), jnp.float32)
            for shift in range(8):
                rolled = strip if shift == 0 else pltpu.roll(strip, 160 - shift, 0)
                for k in range(31):
                    if (k + 1) % 8 == shift:
                        first = (k + 1) // 8 * 8
                        total = total + T[pl.ds(k, 1), lanes] * rolled[first : first + 128]
            CV[:, lanes] = total.astype(jnp.bfloat16).astype(jnp.float32)

    for m in range(4):
        event(f"p1_{m}")(lambda m=m: p1(m))
        event(f"c_{m}")(lambda m=m: compute(m))
        for T_ in "AB":
            event(f"p2{T_}_{m}")(lambda m=m, T_=T_: p2(T_, m))
            event(f"d{T_}_{m}")(lambda m=m, T_=T_: d2d(T_, m))
            for d in "+-":
                event(f"p1r{T_}{m}{d}")(lambda m=m, T_=T_, d=d: p1r(T_, m, d))
                event(f"p2r{T_}{m}{d}")(lambda m=m, T_=T_, d=d: p2r(T_, m, d))

    for name in ORDER:
        with jax.named_scope(name):
            events[name]()

    assert len(groups) == NSEM and len(kinds) == 13, (len(groups), len(kinds))

    def norm(i, carry):
        rows = pl.ds(pl.multiple_of(i * 16, 16), 16)
        v = CV[rows, :]
        mean = jnp.mean(v, axis=-1, keepdims=True)
        cen = v - mean
        var = jnp.mean(cen * cen, axis=-1, keepdims=True)
        n = cen * lax.rsqrt(var + 1e-05) * gain[...] + bias[...]
        ACT[rows, :] = (n * jax.nn.sigmoid(n)).astype(jnp.bfloat16)
        return carry

    with jax.named_scope("norm"):
        lax.fori_loop(0, 8, norm, 0)

    with jax.named_scope("out_rows"):
        arrived("od", O.at[:, 1 - c])

    def emit(j):
        cols = pl.ds(pl.multiple_of(j * 512, 512), 512)
        return pltpu.make_async_copy(out.at[:, cols], result.at[:, cols], lsem.at[7 + j])

    def project(j, carry):
        acc = None
        zs = pl.ds(j * 4, 4)
        for i in range(4):
            w = jnp.concatenate([O[i, 0, zs].reshape(512, 128), O[i, 1, zs].reshape(512, 128)], axis=1)
            part = lax.dot_general(
                ACT[:, 256 * i : 256 * i + 256], w, NT, preferred_element_type=jnp.float32
            )
            acc = part if acc is None else acc + part
        out[:, pl.ds(pl.multiple_of(j * 512, 512), 512)] = acc.astype(jnp.bfloat16)
        emit(j).start()
        return carry

    with jax.named_scope("project"):
        lax.fori_loop(0, 4, project, 0)
    with jax.named_scope("outdma"):
        for j in range(4):
            emit(j).wait()

    with jax.named_scope("drain"):
        sent("p2", W.at[pl.ds(0, 2), c])
        sent("p2r", W.at[0, c])
        sent("p1", W.at[0, c, pl.ds(0, 2)])
        sent("p1r", W.at[0, c, 0])
        sent("d2d", W.at[:, c])
        sent("s2", W.at[0, c, 0, pl.ds(0, 3)])
        sent("s1", W.at[0, c, 0, pl.ds(0, 3), 0])
        sent("ox", O.at[0, c, 0, pl.ds(0, 3)])
        sent("oy", O.at[pl.ds(0, 3), c, 0])
        sent("ring", O.at[:, c, pl.ds(0, 15)])
        sent("od", O.at[:, c])

    @pl.when(sp < 63)
    def _():
        halo_r.wait_send()

    @pl.when(sp > 0)
    def _():
        halo_l.wait_send()


def on_device(tokens, w_value, w_gate, w_out, conv_taps, norm_gain, norm_bias):
    hbm = pl.BlockSpec(memory_space=pltpu.HBM)
    vmem = pl.BlockSpec(memory_space=pltpu.VMEM)
    mixed = pl.pallas_call(
        kernel,
        out_shape=jax.ShapeDtypeStruct((128, 2048), jnp.bfloat16),
        in_specs=[hbm] * 7,
        out_specs=hbm,
        scratch_shapes=[
            pltpu.VMEM((128, 2048), jnp.bfloat16),
            pltpu.VMEM((4, 2, 4, 4, 4, 2, 16, 256), jnp.bfloat16),
            pltpu.VMEM((4, 2, 16, 4, 32, 128), jnp.bfloat16),
            pltpu.VMEM((160, 2048), jnp.bfloat16),
            pltpu.VMEM((31, 1024), jnp.bfloat16),
            pltpu.VMEM((31, 1024), jnp.float32),
            pltpu.VMEM((1, 1024), jnp.float32),
            pltpu.VMEM((1, 1024), jnp.float32),
            pltpu.VMEM((128, 1024), jnp.float32),
            pltpu.VMEM((128, 1024), jnp.bfloat16),
            pltpu.SemaphoreType.DMA((13,)),
            pltpu.SemaphoreType.DMA((NSEM,)),
            pltpu.SemaphoreType.DMA((11,)),
        ],
        compiler_params=pltpu.CompilerParams(
            collective_id=0, has_side_effects=True, vmem_limit_bytes=67043328
        ),
    )(
        tokens[0],
        w_value.T,
        w_gate.T,
        w_out.T,
        conv_taps.T,
        norm_gain[None, :],
        norm_bias[None, :],
    )
    return mixed[None]


def solution(mesh):
    in_specs = (P("dp", "sp", None), P("dp", "sp"), P("dp", "sp"), P("dp", "sp"), P(), P(), P())
    out_specs = P("dp", "sp", None)
    return jax.shard_map(
        on_device, mesh=mesh, in_specs=in_specs, out_specs=out_specs, check_vma=False
    )
```

time: 81.5 us -> 68.5 us (0.84)
  Pallas kernels: 75.7 us -> 66.4 us
  local copies, waits for them, and re-layouts: 5.46 us -> 1.88 us
    pallas_call x1, Pallas kernels: 75.7 us -> 66.4 us  [on_device(): pl.pallas_call(kernel, out_shape=jax.ShapeDtypeStruct((128, 2048), jnp.bf...]
    unnamed x15 -> x1, local copies, waits for them, and re-layouts: 5.46 us -> 1.88 us
where the time goes in v2:
time: 68.5 us; the launch traced here: 68.3 us
  Pallas kernels  66.4 us (97%)
  local copies, waits for them, and re-layouts  1.88 us (3%)
    pallas_call x1, Pallas kernels, on_device(): pl.pallas_call(kernel, out_shape=jax.ShapeDtypeStruct((128, 2048), jnp.bf...  66.4 us
    unnamed x1, local copies, waits for them, and re-layouts  1.88 us

profile of v2, /device:TPU:1, one launch (start us, length us, event | category | flops | bytes accessed | tf_op | source)
XLA Modules:
  0.0 68.3 jit_solution(2606160422815920019)
XLA Ops:
  0.0 66.4 %shard_map.73 = bf16[128,2048]{1,0:T(8,128)(2,1)} custom-call(bf16[128,2048]{1,0:T(8,128)(2,1)} %bitcast.9, bf16[16,256]{1,0:T(8,128)(2,1)} %bitcast.11, bf16[16,256]{1,0:T(8,128)(2,1)} %bitcast.12, bf16[32,128]{1,0:T(8,128)(2,1)} %bitcast.13, bf16[31,1024]{1,0:T(8,128)(2,1)} %bitcast.10, f32[1,1024]{1,0:T(1,128)} %bitcast.14, f32[1,1024]{1,0:T(1,128)} %bitcast.15), custom_call_target="tpu_custom_call" | custom-call | tf_op jit(solution)/shard_map/pallas_call | solution.py:369
  66.4 1.9 %copy.9 = bf16[1,128,2048]{2,1,0:T(8,128)(2,1)} copy(bf16[1,128,2048]{2,1,0:T(8,128)(2,1)} %bitcast.8) | data formatting | bytes 1048576

commit v3 on v2

--- a/solution.py
+++ b/solution.py
@@ -6,21 +6,22 @@
 from jax.sharding import PartitionSpec as P
 
 MESH = pl.DeviceIdType.MESH
-NSEM = 100
+NSEM = 96
 ORDER = [
-    "ox", "s1", "halo", "oxr+", "oxr-", "oy", "p1_0", "s1l", "s1r", "oyr+", "oyr-", "p1rA0+", "p1rA0-",
-    "p1rB0+", "p1rB0-", "g0", "p2A_0", "p1_1", "s1rr", "p2B_0", "p1_2", "p1rA1+", "g1_0", "p2rA0+", "g1_1",
-    "p1rB1+", "p1rB1-", "g1_3", "p2rA0-", "p2rB0+", "p1rA2-", "p1rA2+", "p1rB2+", "g1_2", "g2_0", "p1rA1-",
-    "p1rB2-", "p1_3", "g2_3", "p2B_1", "g2_1", "dA_0", "g2_2", "p2A_2", "g3_0", "p2rB0-", "g3_3", "p1rA3-",
-    "p2B_2", "p2A_1", "g3_1", "p1rA3+", "p2rB1-", "g3_2", "p1rB3+", "p1rB3-", "g4_0", "dB_0", "g4_3",
-    "p2rA2+", "p2rB1+", "p2A_3", "g4_1", "p2rA1+", "p2rA1-", "g4_2", "p2B_3", "p2rB2-", "g5_3", "g5_0",
-    "p2rA2-", "g5_1", "p2rB2+", "p2rA3-", "p2rA3+", "g5_2", "p2rB3+", "p2rB3-", "c_0", "dB_1", "dA_1", "g6_3",
-    "g6_0", "dA_2", "g6_1", "dB_2", "g6_2", "dA_3", "dB_3", "g7_3", "c_1", "g7_0", "g7_1", "c_2", "g7_2",
-    "g8_3", "c_3", "g8_1", "g8_0", "g8_2",
+    "s1", "ox", "halo", "oy", "p1_0", "s1l", "s1r", "p1rA0-", "g0", "p1rA0+", "s1rr", "p1rB0+", "p2A_0",
+    "p1rB0-", "p2B_0", "p1_1", "g1_0", "g1_1", "p1_2", "g1_3", "g1_2", "p2rA0-", "p2rA0+", "p1rB1+", "g2_0",
+    "p2rB0-", "p1rA1+", "p1rA1-", "g2_1", "p1_3", "p1rB2+", "p1rB1-", "g2_3", "g2_2", "p1rA2-", "p1rA2+",
+    "p1rB2-", "g3_0", "p2rB0+", "g3_1", "g3_3", "p1rA3+", "p2A_1", "g3_2", "dA_0", "p2B_1", "p1rA3-", "g4_0",
+    "g4_1", "p1rB3+", "p1rB3-", "g4_3", "g4_2", "p2A_2", "p2B_2", "g5_0", "p2rA1+", "p2rA1-", "g5_1",
+    "p2rB1+", "p2A_3", "p2rB1-", "dB_0", "p2B_3", "g5_3", "g5_2", "g6_0", "p2rB2+", "p2rB2-", "p2rA2-",
+    "g6_1", "p2rA2+", "p2rA3+", "p2rA3-", "g6_3", "p2rB3+", "g6_2", "p2rB3-", "dA_1", "c_0", "g7_0", "dB_1",
+    "g7_1", "dB_2", "dA_2", "g7_3", "g7_2", "dA_3", "dB_3", "c_1", "c_2", "g8_1", "g8_3", "g8_0", "g8_2",
+    "c_3",
 ]
-SENDS = {"ox+": "ox", "ox-": "ox", "oxr": "ox", "oy+": "oy", "oy-": "oy", "oyr": "oy",
+SENDS = {"ox": "ox", "oy": "oy",
          "s1+": "s1", "s1-": "s1", "s1r": "s1", "od": "od"}
 FIRST = 0
+DIRECT = (0,)
 NT = (((1,), (1,)), ((), ()))
 
 
@@ -63,6 +64,7 @@
     barrier = pltpu.get_barrier_semaphore()
     partners = [dev(x=xl), dev(x=xr), dev(y=yl), dev(y=yr), dev(z=zl), dev(z=zr), dev(z=z4l), dev(z=z4r)]
     partners += [dev(z=p) for p in peers]
+    partners += [dev(x=mod(x + 2, 4)), dev(y=mod(y + 2, 4))]
     partners += [dev(c=1 - c), {"sp": prev, "dp": dp}, {"sp": nxt, "dp": dp}]
     for p in partners:
         pl.semaphore_signal(barrier, inc=1, device_id=p, device_id_type=MESH)
@@ -127,34 +129,14 @@
 
     @event("ox")
     def _():
-        send("ox+", O.at[x, c, z, y], dev(x=xr))
-        send("ox-", O.at[x, c, z, y], dev(x=xl))
-
-    @event("oxr+")
-    def _():
-        arrived("ox+", O.at[x, c, z, y])
-        send("oxr", O.at[xl, c, z, y, pl.ds(0, 16)], dev(x=xr))
-
-    @event("oxr-")
-    def _():
-        arrived("ox-", O.at[x, c, z, y])
-        send("oxr", O.at[xr, c, z, y, pl.ds(16, 16)], dev(x=xl))
+        for d in (1, 3, 2):
+            send("ox", O.at[x, c, z, y], dev(x=mod(x + d, 4)))
 
     @event("oy")
     def _():
-        arrived("oxr", O.at[x, c, z, y])
-        send("oy+", O.at[:, c, z, y], dev(y=yr))
-        send("oy-", O.at[:, c, z, y], dev(y=yl))
-
-    @event("oyr+")
-    def _():
-        arrived("oy+", O.at[:, c, z, y])
-        send("oyr", O.at[lo, c, z, yl], dev(y=yr))
-
-    @event("oyr-")
-    def _():
-        arrived("oy-", O.at[:, c, z, y])
-        send("oyr", O.at[hi, c, z, yr], dev(y=yl))
+        arrived("ox", O.at[pl.ds(0, 3), c, z, y])
+        for d in (1, 3, 2):
+            send("oy", O.at[:, c, z, y], dev(y=mod(y + d, 4)))
 
     stepped = [0] * 9
 
@@ -174,7 +156,7 @@
 
     @event("g0")
     def _():
-        arrived("oyr", O.at[:, c, z, y])
+        arrived("oy", O.at[:, c, z, pl.ds(0, 3)])
         for h in range(4):
             ring(0, h)
 
@@ -232,10 +214,13 @@
                 send(("p1", T, m, d), part(T, m, "o"), ring1[T][d])
             for d in "+-":
                 send(("p2", T, m, d), part(T, m, "o"), ring2[T][d])
+            if m in DIRECT:
+                send(("p1r", T, m), part(T, m, "o"), dev(y=mod(y + 2, 4)) if T == "A" else dev(x=mod(x + 2, 4)))
 
     def p1r(T, m, d):
         arrived(("p1", T, m, d), part(T, m, "o"))
-        send(("p1r", T, m), part(T, m, d, half[d]), ring1[T][d])
+        if m not in DIRECT:
+            send(("p1r", T, m), part(T, m, d, half[d]), ring1[T][d])
         for e in "+-":
             send(("p2", T, m, e), part(T, m, d), ring2[T][e])
 

time: 68.5 us -> 62 us (0.905)
  Pallas kernels: 66.4 us -> 60 us
    pallas_call x1, Pallas kernels: 66.4 us -> 60 us  [on_device(): pl.pallas_call(kernel, out_shape=jax.ShapeDtypeStruct((128, 2048), jnp.bf...]
where the time goes in v3:
time: 62 us; the launch traced here: 61.9 us
  Pallas kernels  60 us (97%)
  local copies, waits for them, and re-layouts  1.88 us (3%)
    pallas_call x1, Pallas kernels, on_device(): pl.pallas_call(kernel, out_shape=jax.ShapeDtypeStruct((128, 2048), jnp.bf...  60 us
    unnamed x1, local copies, waits for them, and re-layouts  1.88 us

profile of v3, /device:TPU:1, one launch (start us, length us, event | category | flops | bytes accessed | tf_op | source)
XLA Modules:
  0.0 61.9 jit_solution(5166798720401660302)
XLA Ops:
  0.0 60.0 %shard_map.73 = bf16[128,2048]{1,0:T(8,128)(2,1)} custom-call(bf16[128,2048]{1,0:T(8,128)(2,1)} %bitcast.9, bf16[16,256]{1,0:T(8,128)(2,1)} %bitcast.11, bf16[16,256]{1,0:T(8,128)(2,1)} %bitcast.12, bf16[32,128]{1,0:T(8,128)(2,1)} %bitcast.13, bf16[31,1024]{1,0:T(8,128)(2,1)} %bitcast.10, f32[1,1024]{1,0:T(1,128)} %bitcast.14, f32[1,1024]{1,0:T(1,128)} %bitcast.15), custom_call_target="tpu_custom_call" | custom-call | tf_op jit(solution)/shard_map/pallas_call | solution.py:354
  60.0 1.9 %copy.9 = bf16[1,128,2048]{2,1,0:T(8,128)(2,1)} copy(bf16[1,128,2048]{2,1,0:T(8,128)(2,1)} %bitcast.8) | data formatting | bytes 1048576

commit v4 on v3

--- a/solution.py
+++ b/solution.py
@@ -14,7 +14,7 @@
     "p1rB2-", "g3_0", "p2rB0+", "g3_1", "g3_3", "p1rA3+", "p2A_1", "g3_2", "dA_0", "p2B_1", "p1rA3-", "g4_0",
     "g4_1", "p1rB3+", "p1rB3-", "g4_3", "g4_2", "p2A_2", "p2B_2", "g5_0", "p2rA1+", "p2rA1-", "g5_1",
     "p2rB1+", "p2A_3", "p2rB1-", "dB_0", "p2B_3", "g5_3", "g5_2", "g6_0", "p2rB2+", "p2rB2-", "p2rA2-",
-    "g6_1", "p2rA2+", "p2rA3+", "p2rA3-", "g6_3", "p2rB3+", "g6_2", "p2rB3-", "dA_1", "c_0", "g7_0", "dB_1",
+    "g6_1", "dA_1", "dB_1", "p2rA2+", "p2rA3+", "p2rA3-", "g6_3", "p2rB3+", "g6_2", "p2rB3-", "c_0", "g7_0",
     "g7_1", "dB_2", "dA_2", "g7_3", "g7_2", "dA_3", "dB_3", "c_1", "c_2", "g8_1", "g8_3", "g8_0", "g8_2",
     "c_3",
 ]
@@ -26,8 +26,8 @@
 
 
 def kernel(
-    tok, wv, wg, wo, taps_in, gain_in, bias_in, result,
-    out, W, O, X, TB, T, gain, bias, CV, ACT, ssem, rsem, lsem,
+    tok, wv, wg, wo, taps_in, gain_in, bias_in, out,
+    W, O, X, TB, T, gain, bias, CV, ACT, ssem, rsem, lsem,
 ):
     sp = lax.axis_index("sp")
     dp = lax.axis_index("dp")
@@ -144,9 +144,9 @@
         zo, zp = mod(z - s, 16), mod(z + s, 16)
         if s > 0:
             arrived(("ring", s - 1, h), O.at[:, c, z, pl.ds(0, 2 if s < 8 else 1)])
-        if s < 8:
+        if s < 7 or (s == 7 and h < 2):
             send(("ring", s, h), O.at[:, c, zo, h], dev(z=zr))
-        if s < 7:
+        if s < 7 or (s == 7 and h >= 2):
             send(("ring", s, h), O.at[:, c, zp, h], dev(z=zl))
         stepped[s] += 1
         if stepped[s] == 4:
@@ -298,14 +298,10 @@
         return carry
 
     with jax.named_scope("norm"):
-        lax.fori_loop(0, 8, norm, 0)
+        lax.fori_loop(0, 8, norm, 0, unroll=4)
 
     with jax.named_scope("out_rows"):
         arrived("od", O.at[:, 1 - c])
-
-    def emit(j):
-        cols = pl.ds(pl.multiple_of(j * 512, 512), 512)
-        return pltpu.make_async_copy(out.at[:, cols], result.at[:, cols], lsem.at[7 + j])
 
     def project(j, carry):
         acc = None
@@ -317,14 +313,10 @@
             )
             acc = part if acc is None else acc + part
         out[:, pl.ds(pl.multiple_of(j * 512, 512), 512)] = acc.astype(jnp.bfloat16)
-        emit(j).start()
         return carry
 
     with jax.named_scope("project"):
         lax.fori_loop(0, 4, project, 0)
-    with jax.named_scope("outdma"):
-        for j in range(4):
-            emit(j).wait()
 
     with jax.named_scope("drain"):
         sent("p2", W.at[pl.ds(0, 2), c])
@@ -355,9 +347,8 @@
         kernel,
         out_shape=jax.ShapeDtypeStruct((128, 2048), jnp.bfloat16),
         in_specs=[hbm] * 7,
-        out_specs=hbm,
+        out_specs=vmem,
         scratch_shapes=[
-            pltpu.VMEM((128, 2048), jnp.bfloat16),
             pltpu.VMEM((4, 2, 4, 4, 4, 2, 16, 256), jnp.bfloat16),
             pltpu.VMEM((4, 2, 16, 4, 32, 128), jnp.bfloat16),
             pltpu.VMEM((160, 2048), jnp.bfloat16),
@@ -369,19 +360,18 @@
             pltpu.VMEM((128, 1024), jnp.bfloat16),
             pltpu.SemaphoreType.DMA((13,)),
             pltpu.SemaphoreType.DMA((NSEM,)),
-            pltpu.SemaphoreType.DMA((11,)),
+            pltpu.SemaphoreType.DMA((7,)),
         ],
         compiler_params=pltpu.CompilerParams(
-            collective_id=0, has_side_effects=True, vmem_limit_bytes=67043328
+            collective_id=0, has_side_effects=True, vmem_limit_bytes=50000000
         ),
     )(
-        tokens[0],
-        w_value.T,
-        w_gate.T,
-        w_out.T,
-        conv_taps.T,
-        norm_gain[None, :],
-        norm_bias[None, :],
+        *[
+            pltpu.with_memory_space_constraint(a, pltpu.HBM)
+            for a in (
+                tokens[0], w_value.T, w_gate.T, w_out.T, conv_taps.T, norm_gain[None, :], norm_bias[None, :],
+            )
+        ]
     )
     return mixed[None]
 

time: 62 us -> 59.3 us (0.956)
  Pallas kernels: 60 us -> 58.4 us
  local copies, waits for them, and re-layouts: 1.88 us -> 0.8 us
    pallas_call x1, Pallas kernels: 60 us -> 58.4 us  [on_device(): pl.pallas_call(kernel, out_shape=jax.ShapeDtypeStruct((128, 2048), jnp.bf...]
    unnamed x1, local copies, waits for them, and re-layouts: 1.88 us -> 0.8 us
where the time goes in v4:
time: 59.3 us; the launch traced here: 59.2 us
  Pallas kernels  58.4 us (98%)
  local copies, waits for them, and re-layouts  0.8 us (1%)
    pallas_call x1, Pallas kernels, on_device(): pl.pallas_call(kernel, out_shape=jax.ShapeDtypeStruct((128, 2048), jnp.bf...  58.4 us

profile of v4, /device:TPU:1, one launch (start us, length us, event | category | flops | bytes accessed | tf_op | source)
XLA Modules:
  0.0 59.2 jit_solution(12941849198991146396)
XLA Ops:
  0.0 58.4 %shard_map.73 = bf16[128,2048]{1,0:T(8,128)(2,1)S(1)} custom-call(bf16[128,2048]{1,0:T(8,128)(2,1)} %bitcast.9, bf16[16,256]{1,0:T(8,128)(2,1)} %bitcast.11, bf16[16,256]{1,0:T(8,128)(2,1)} %bitcast.12, bf16[32,128]{1,0:T(8,128)(2,1)} %bitcast.13, bf16[31,1024]{1,0:T(8,128)(2,1)} %bitcast.10, f32[1,1024]{1,0:T(1,128)} %bitcast.14, f32[1,1024]{1,0:T(1,128)} %bitcast.15), custom_call_target="tpu_custom_call" | custom-call | tf_op jit(solution)/shard_map/pallas_call | solution.py:346
  58.4 0.8 %copy.9 = bf16[1,128,2048]{2,1,0:T(8,128)(2,1)} copy(bf16[1,128,2048]{2,1,0:T(8,128)(2,1)S(1)} %bitcast.8) | data formatting | bytes 1048576

commit v5 on v4

--- a/solution.py
+++ b/solution.py
@@ -298,7 +298,7 @@
         return carry
 
     with jax.named_scope("norm"):
-        lax.fori_loop(0, 8, norm, 0, unroll=4)
+        lax.fori_loop(0, 8, norm, 0, unroll=8)
 
     with jax.named_scope("out_rows"):
         arrived("od", O.at[:, 1 - c])
@@ -316,7 +316,7 @@
         return carry
 
     with jax.named_scope("project"):
-        lax.fori_loop(0, 4, project, 0)
+        lax.fori_loop(0, 4, project, 0, unroll=4)
 
     with jax.named_scope("drain"):
         sent("p2", W.at[pl.ds(0, 2), c])

time: 59.3 us -> 58.9 us (level)
  no operation moved by 1% of the time
where the time goes in v5:
time: 58.9 us; the launch traced here: 58.7 us
  Pallas kernels  57.9 us (98%)
  local copies, waits for them, and re-layouts  0.8 us (1%)
    pallas_call x1, Pallas kernels, on_device(): pl.pallas_call(kernel, out_shape=jax.ShapeDtypeStruct((128, 2048), jnp.bf...  57.9 us

profile of v5, /device:TPU:1, one launch (start us, length us, event | category | flops | bytes accessed | tf_op | source)
XLA Modules:
  0.0 58.7 jit_solution(18229722100903194024)
XLA Ops:
  0.0 57.9 %shard_map.73 = bf16[128,2048]{1,0:T(8,128)(2,1)S(1)} custom-call(bf16[128,2048]{1,0:T(8,128)(2,1)} %bitcast.9, bf16[16,256]{1,0:T(8,128)(2,1)} %bitcast.11, bf16[16,256]{1,0:T(8,128)(2,1)} %bitcast.12, bf16[32,128]{1,0:T(8,128)(2,1)} %bitcast.13, bf16[31,1024]{1,0:T(8,128)(2,1)} %bitcast.10, f32[1,1024]{1,0:T(1,128)} %bitcast.14, f32[1,1024]{1,0:T(1,128)} %bitcast.15), custom_call_target="tpu_custom_call" | custom-call | tf_op jit(solution)/shard_map/pallas_call | solution.py:346
  57.9 0.8 %copy.9 = bf16[1,128,2048]{2,1,0:T(8,128)(2,1)} copy(bf16[1,128,2048]{2,1,0:T(8,128)(2,1)S(1)} %bitcast.8) | data formatting | bytes 1048576

commit v6 on v5

--- a/solution.py
+++ b/solution.py
@@ -15,7 +15,7 @@
     "g4_1", "p1rB3+", "p1rB3-", "g4_3", "g4_2", "p2A_2", "p2B_2", "g5_0", "p2rA1+", "p2rA1-", "g5_1",
     "p2rB1+", "p2A_3", "p2rB1-", "dB_0", "p2B_3", "g5_3", "g5_2", "g6_0", "p2rB2+", "p2rB2-", "p2rA2-",
     "g6_1", "dA_1", "dB_1", "p2rA2+", "p2rA3+", "p2rA3-", "g6_3", "p2rB3+", "g6_2", "p2rB3-", "c_0", "g7_0",
-    "g7_1", "dB_2", "dA_2", "g7_3", "g7_2", "dA_3", "dB_3", "c_1", "c_2", "g8_1", "g8_3", "g8_0", "g8_2",
+    "g7_1", "dB_2", "dA_2", "g7_3", "g7_2", "dA_3", "dB_3", "c_1", "g8_1", "g8_3", "g8_0", "g8_2", "c_2",
     "c_3",
 ]
 SENDS = {"ox": "ox", "oy": "oy",

time: 58.9 us -> 58.6 us (level)
  no operation moved by 1% of the time
where the time goes in v6:
time: 58.6 us; the launch traced here: 58.4 us
  Pallas kernels  57.6 us (98%)
  local copies, waits for them, and re-layouts  0.8 us (1%)
    pallas_call x1, Pallas kernels, on_device(): pl.pallas_call(kernel, out_shape=jax.ShapeDtypeStruct((128, 2048), jnp.bf...  57.6 us

profile of v6, /device:TPU:1, one launch (start us, length us, event | category | flops | bytes accessed | tf_op | source)
XLA Modules:
  0.0 58.4 jit_solution(14500471156957767050)
XLA Ops:
  0.0 57.6 %shard_map.73 = bf16[128,2048]{1,0:T(8,128)(2,1)S(1)} custom-call(bf16[128,2048]{1,0:T(8,128)(2,1)} %bitcast.9, bf16[16,256]{1,0:T(8,128)(2,1)} %bitcast.11, bf16[16,256]{1,0:T(8,128)(2,1)} %bitcast.12, bf16[32,128]{1,0:T(8,128)(2,1)} %bitcast.13, bf16[31,1024]{1,0:T(8,128)(2,1)} %bitcast.10, f32[1,1024]{1,0:T(1,128)} %bitcast.14, f32[1,1024]{1,0:T(1,128)} %bitcast.15), custom_call_target="tpu_custom_call" | custom-call | tf_op jit(solution)/shard_map/pallas_call | solution.py:346
  57.6 0.8 %copy.9 = bf16[1,128,2048]{2,1,0:T(8,128)(2,1)} copy(bf16[1,128,2048]{2,1,0:T(8,128)(2,1)S(1)} %bitcast.8) | data formatting | bytes 1048576
